TPU v7x, 512 devices: a whole 4x4x16 slice. The times are simulated.
512 devices in a mesh: ep: 128 (over z, x, core), tp: 4 (over y).
Axes of the slice: x: 4, y: 4, z: 16, core: 2. Of those that a mesh axis runs over, the one named last changes fastest.
Arguments:
- tokens: bfloat16 [1024, 1024], P('ep'), may hold values from -6 to 6
- kv_cache: bfloat16 [1024, 4, 1024, 128], P('ep', 'tp'), may hold values from -6 to 6
- lengths: int32 [1024], P('ep'), may hold values from 256 to 1024
- w_query: bfloat16 [1024, 512], P(None, 'tp'), may hold values from -0.1875 to 0.1875
- w_key: bfloat16 [1024, 256], P(None, 'tp'), may hold values from -0.1875 to 0.1875
- w_value: bfloat16 [1024, 256], P(None, 'tp'), may hold values from -0.1875 to 0.1875
- break_bias: float32 [8], P('tp'), may hold values from -7.5 to -3.5
- head_gain: float32 [512], P('tp'), may hold values from 0.1 to 1.9
- w_output: bfloat16 [512, 1024], P('tp'), may hold values from -0.25 to 0.25
- attn_norm_gain: float32 [1024], replicated, may hold values from 0.1 to 1.9
- w_router: bfloat16 [1024, 16], replicated, may hold values from -0.1875 to 0.1875
- routes: int32 [1024, 2], P('ep'), may hold values from 0 to 15, all different within a row; in each aligned block of 8 rows (0 to 7, 8 to 15, ...) at most 2 rows name the same one
- expert_gate: bfloat16 [1024, 57344], P(None, ('ep', 'tp')), may hold values from -0.1875 to 0.1875
- expert_up: bfloat16 [1024, 57344], P(None, ('ep', 'tp')), may hold values from -0.1875 to 0.1875
- expert_down: bfloat16 [57344, 1024], P(('ep', 'tp')), may hold values from -0.09375 to 0.09375
- dense_gate: bfloat16 [1024, 2816], P(None, 'ep'), may hold values from -0.1875 to 0.1875
- dense_up: bfloat16 [1024, 2816], P(None, 'ep'), may hold values from -0.1875 to 0.1875
- dense_down: bfloat16 [2816, 1024], P('ep', 'tp'), may hold values from -0.109375 to 0.109375
- mix_gate: bfloat16 [1024], replicated, may hold values from -0.1875 to 0.1875
- ffn_norm_gain: float32 [1024], P('tp'), may hold values from 0.1 to 1.9
Outputs:
- layer_out: bfloat16 [1024, 1024], P('ep', 'tp')
- new_kv: bfloat16 [1024, 4, 128], P('ep', 'tp')
Inputs may be any that keep to these rules, and one draw needn't show every extreme that they name: lengths[b] is the number of valid cached positions of sequence b and the new token's position. `routes`: each row names 2 different experts. Among the rows of one index of ep (aligned blocks of 8 rows) no expert is named more than 2 times, a bound that some block reaches.
All inputs are finite; a program needn't handle non-finite values.
Results may differ from a plain program's by a relative error of at most 0.012.
Values may be sent and summed in bfloat16 or wider, within the bound.
A program may use at most 128 MiB of HBM per device.

v0:
```python
import jax
import jax.numpy as jnp
from jax import lax
from jax.sharding import Mesh
from jax.sharding import PartitionSpec as P

FE = 3584
CAP = 2
EP = ("ep_0", "ep_1", "ep_2")
EP_TP = ("ep_0", "ep_1", "ep_2", "tp")
RESIDUAL_SCALE = 8.0**0.25
PRECISE = lax.Precision.HIGHEST


def from_everyone(shard, axis):
    copies = jnp.broadcast_to(shard, (lax.axis_size(axis), *shard.shape))
    return lax.all_to_all(copies, axis, split_axis=0, concat_axis=0, tiled=True)


def of_everyone(shard, axis):
    everything = from_everyone(shard, axis)
    return jnp.sum(everything.astype(jnp.float32), axis=0)


def cut_along(shard, dim, peers):
    shape = shard.shape
    tiles = shard.reshape(*shape[:dim], peers, shape[dim] // peers, *shape[dim + 1 :])
    return jnp.moveaxis(tiles, dim, 0)


def summed_on_arrival(shard, axis, dim):
    peers = lax.axis_size(axis)
    tiles = lax.all_to_all(cut_along(shard, dim, peers), axis, 0, 0, tiled=True)
    return jnp.sum(tiles.astype(jnp.float32), axis=0)


def joined_along(tiles, dim):
    tiles = jnp.moveaxis(tiles, 0, dim)
    shape = tiles.shape
    return tiles.reshape(*shape[:dim], shape[dim] * shape[dim + 1], *shape[dim + 2 :])


def stacked_from(shard, axes, sequence):
    tiles = shard[None]
    for k in sequence:
        tiles = lax.all_gather(tiles, axes[k], axis=0, tiled=True)
    block = [lax.axis_size(axes[k]) for k in reversed(sequence)]
    tiles = tiles.reshape(*block, *shard.shape)
    turned = sorted(range(len(sequence)), key=lambda place: sequence[len(sequence) - 1 - place])
    return tiles.transpose(*turned, *range(len(sequence), tiles.ndim)).reshape(-1, *shard.shape)


def gathered_by_axis(shard, axes, sequence, dim):
    return joined_along(stacked_from(shard, axes, sequence), dim)


def of_everyone_2(shard, axis):
    return from_everyone(shard, axis).sum(axis=0)


def together(arrays, axis):
    ends = [0]
    for a in arrays:
        ends.append(ends[-1] + a.size)
    so_far = of_everyone_2(jnp.concatenate([a.ravel() for a in arrays]), axis)
    return tuple((so_far[b:e].reshape(a.shape) for a, b, e in zip(arrays, ends, ends[1:])))


def layer_norm(values, gain):
    centre = jnp.mean(values, axis=-1, keepdims=True)
    centred = values - centre
    spread = jnp.mean(centred * centred, axis=-1, keepdims=True)
    return centred * lax.rsqrt(spread + 1e-05) * gain


def stick_weights(scores, visible):
    survive = jnp.where(visible, jax.nn.log_sigmoid(-scores), 0.0)
    remaining = lax.cumsum(survive, axis=3, reverse=True) - survive
    return jnp.where(visible, jnp.exp(jax.nn.log_sigmoid(scores) + remaining), 0.0)


def body(
    tokens,
    kv_cache,
    lengths,
    w_query,
    w_key,
    w_value,
    break_bias,
    head_gain,
    w_output,
    attn_norm_gain,
    w_router,
    routes,
    expert_gate,
    expert_up,
    expert_down,
    dense_gate,
    dense_up,
    dense_down,
    mix_gate,
    ffn_norm_gain,
):
    seq_count = tokens.shape[0]
    model_width = tokens.shape[1]
    key_heads = kv_cache.shape[1]
    positions = kv_cache.shape[2]
    head_dim = kv_cache.shape[3] // 2
    local_heads = w_query.shape[1] // head_dim
    group_size = local_heads // key_heads
    queries = jnp.dot(tokens, w_query, preferred_element_type=jnp.float32).astype(jnp.bfloat16)
    queries = queries.reshape(seq_count, key_heads, group_size, head_dim)
    key_new = jnp.dot(tokens, w_key, preferred_element_type=jnp.float32).astype(jnp.bfloat16)
    value_new = jnp.dot(tokens, w_value, preferred_element_type=jnp.float32).astype(jnp.bfloat16)
    new_kv = jnp.concatenate(
        [
            key_new.reshape(seq_count, key_heads, head_dim),
            value_new.reshape(seq_count, key_heads, head_dim),
        ],
        axis=2,
    )
    cached_keys = kv_cache[..., :head_dim]
    cached_values = kv_cache[..., head_dim:]
    scores = jnp.einsum(
        "bgqd,bgld->bgql", queries, cached_keys, preferred_element_type=jnp.float32
    ) * head_dim ** (-0.5)
    scores = scores + break_bias.reshape(1, key_heads, group_size, 1)
    visible = lax.broadcasted_iota(jnp.int32, (seq_count, 1, 1, positions), 3) < lengths.reshape(
        seq_count, 1, 1, 1
    )
    weights = stick_weights(scores, visible).astype(jnp.bfloat16)
    blended = jnp.einsum(
        "bgql,bgld->bgqd", weights, cached_values, preferred_element_type=jnp.float32
    )
    rescale = lax.rsqrt(jnp.mean(blended * blended, axis=3, keepdims=True) + 1e-06)
    normed = ((blended * rescale).reshape(seq_count, local_heads * head_dim) * head_gain).astype(
        jnp.bfloat16
    )
    partial_out = jnp.dot(normed, w_output, preferred_element_type=jnp.float32)
    attended = of_everyone(partial_out.astype(jnp.bfloat16), "tp").astype(jnp.float32)
    settled = layer_norm(
        RESIDUAL_SCALE * tokens.astype(jnp.float32) + attended, attn_norm_gain
    ).astype(jnp.bfloat16)
    experts = w_router.shape[1]
    top_count = routes.shape[1]
    logits = jnp.dot(settled, w_router, preferred_element_type=jnp.float32)
    chosen = routes[:, :, None] == lax.broadcasted_iota(
        jnp.int32, (seq_count, top_count, experts), 2
    )
    picked = jnp.sum(jnp.where(chosen, logits[:, None, :], 0.0), axis=2)
    route_weight = jax.nn.sigmoid(picked - picked[:, ::-1])
    assigned = chosen.reshape(seq_count * top_count, experts).astype(jnp.int32)
    before = jnp.cumsum(assigned, axis=0) - assigned
    slot_index = jnp.sum(before * assigned, axis=1)
    slot_hits = (
        slot_index[:, None] == lax.broadcasted_iota(jnp.int32, (seq_count * top_count, CAP), 1)
    ).astype(jnp.int32)
    placement = (assigned[:, :, None] * slot_hits[:, None, :]).reshape(
        seq_count, top_count, experts * CAP
    )
    selector = jnp.sum(placement, axis=1).astype(jnp.bfloat16)
    weighted = jnp.sum(placement.astype(jnp.float32) * route_weight[:, :, None], axis=1)
    buffer = lax.dot_general(
        selector, settled, (((0,), (0,)), ((), ())), preferred_element_type=jnp.float32
    )
    buffer = buffer.astype(jnp.bfloat16).reshape(experts, CAP, model_width)
    hosts = lax.axis_size(EP)
    tp_size = lax.axis_size("tp")
    per_host = 1
    outgoing = jnp.repeat(buffer, hosts // experts, axis=0).reshape(hosts, 1, CAP, model_width)
    columns = expert_gate.shape[1]
    block_index = lax.axis_index(EP_TP)
    own_expert = block_index * columns // FE
    local_slot = own_expert - lax.axis_index(EP) * experts // hosts
    slice_width = model_width // tp_size
    arrived = lax.all_to_all(outgoing, EP, split_axis=0, concat_axis=0, tiled=True)
    slot_count = arrived.shape[2]
    received = lax.dynamic_index_in_dim(arrived, local_slot, 1, keepdims=False)
    received = received.reshape(hosts * slot_count, model_width)
    gate_pre = jnp.dot(received, expert_gate, preferred_element_type=jnp.float32)
    up_pre = jnp.dot(received, expert_up, preferred_element_type=jnp.float32)
    hidden = (jax.nn.silu(gate_pre) * up_pre).astype(jnp.bfloat16)
    partial_value = jnp.dot(hidden, expert_down, preferred_element_type=jnp.float32)
    partial_value = partial_value.reshape(hosts, 1, slot_count, model_width)
    slot_mask = (lax.broadcasted_iota(jnp.int32, (1, per_host, 1, 1), 1) == local_slot).astype(
        jnp.float32
    )
    summed = summed_on_arrival((partial_value * slot_mask).astype(jnp.bfloat16), "tp", 3)
    returned = lax.all_to_all(
        summed.astype(jnp.bfloat16), EP, split_axis=0, concat_axis=0, tiled=True
    ).astype(summed.dtype)
    host_ids = lax.broadcasted_iota(jnp.int32, (hosts * per_host,), 0)
    host_expert = host_ids // per_host * experts // hosts + host_ids % per_host
    ownership = (
        host_expert[None, :] == lax.broadcasted_iota(jnp.int32, (experts, hosts * per_host), 0)
    ).astype(jnp.float32)
    gathered = jnp.dot(
        ownership, returned.reshape(hosts * per_host, CAP * slice_width), precision=PRECISE
    )
    gathered = gathered.reshape(experts * CAP, slice_width)
    routed = jnp.dot(weighted, gathered, precision=PRECISE)
    column_rank = lax.axis_index("tp")
    own_settled = lax.dynamic_slice_in_dim(settled, column_rank * slice_width, slice_width, 1)
    shard_rows = lax.all_gather(settled, EP, axis=0, tiled=True)
    gate_pre = jnp.dot(shard_rows, dense_gate, preferred_element_type=jnp.float32)
    up_pre = jnp.dot(shard_rows, dense_up, preferred_element_type=jnp.float32)
    dense_hidden = (jax.nn.silu(gate_pre) * up_pre).astype(jnp.bfloat16)
    own_hidden = lax.all_to_all(dense_hidden, EP, split_axis=0, concat_axis=1, tiled=True)
    dense_out = jnp.dot(
        own_hidden,
        gathered_by_axis(dense_down, EP, (0, 1, 2), 0),
        preferred_element_type=jnp.float32,
    )
    mix_weight = jax.nn.sigmoid(jnp.dot(settled, mix_gate, preferred_element_type=jnp.float32))
    combined = (
        RESIDUAL_SCALE * own_settled.astype(jnp.float32) + routed + mix_weight[:, None] * dense_out
    )
    row_sums, squares = together(
        (jnp.sum(combined, axis=1), jnp.sum(combined * combined, axis=1)), "tp"
    )
    row_mean = row_sums / model_width
    row_var = squares / model_width - row_mean * row_mean
    result = (
        (combined - row_mean[:, None]) * lax.rsqrt(row_var[:, None] + 1e-05) * ffn_norm_gain
    ).astype(jnp.bfloat16)
    return (result, new_kv)


def solution(mesh):
    split = Mesh(mesh.devices.reshape(16, 4, 2, mesh.shape["tp"]), ("ep_0", "ep_1", "ep_2", "tp"))
    return jax.shard_map(
        body,
        mesh=split,
        in_specs=(
            P(EP, None),
            P(EP, "tp", None, None),
            P(EP),
            P(None, "tp"),
            P(None, "tp"),
            P(None, "tp"),
            P("tp"),
            P("tp"),
            P("tp", None),
            P(),
            P(),
            P(EP, None),
            P(None, EP_TP),
            P(None, EP_TP),
            P(EP_TP, None),
            P(None, EP),
            P(None, EP),
            P(EP, "tp"),
            P(),
            P("tp"),
        ),
        out_specs=(P(EP, "tp"), P(EP, "tp", None)),
        check_vma=False,
    )
```

profile of v0, /device:TPU:32, one launch (start us, length us, event | category | flops | bytes accessed | tf_op | source)
XLA Modules:
  0.0 307.2 jit_solution(8504936146442683302)
XLA Ops:
  7.2 0.9 iota_compare_fusion
  8.1 1.1 convolution_convert_fusion.4
  9.3 2.3 fusion.31
  11.6 19.8 %reduce-window.6 = f32[8,1,2,8,128]{4,3,2,1,0:T(8,128)S(1)} reduce-window(f32[8,1,2,8,128]{4,3,2,1,0:T(8,128)S(1)} %bitcast.88, f32[]{:T(128)} %constant.108.clone.1), window={size=1x1x1x1x128 pad=0_0x0_0x0_0x0_0x0_127}, to_apply=%region_0.1 | reduce-window | flops 2080768 | bytes 131076 | tf_op jit(solution)/shard_map/reduce-window
  31.5 0.2 copy.65
  31.6 0.3 reduce-window.9
  32.2 1.1 multiply_reduce_fusion.3
  33.5 0.2 convolution_convert_fusion.1
  33.7 0.6 broadcast_in_dim.35
  34.3 4.5 %all-to-all-start = ((bf16[4,8,1024]{2,1,0:T(8,128)(2,1)}), bf16[4,8,1024]{2,1,0:T(8,128)(2,1)S(1)}, u32[]{:S(2)}, u32[]{:S(2)}) async-start(bf16[4,8,1024]{2,1,0:T(8,128)(2,1)} %broadcast_in_dim.35), calls=%async_computation | async-start | bytes 131072 | tf_op jit(solution)/shard_map/all_to_all | solution.py:17
  38.8 34.4 %all-gather.1 = bf16[16,22,256]{2,1,0:T(8,128)(2,1)S(1)} all-gather(bf16[1,22,256]{2,1,0:T(8,128)(2,1)S(1)} %bitcast.90), channel_id=2, replica_groups=mesh['ep_0'=16,'ep_1'=4,'ep_2'=2,'tp'=4] {'ep_0'}, dimensions={0}, use_global_device_ids=true | all-gather | bytes 191488 | tf_op jit(solution)/shard_map/all_gather | solution.py:46
  73.2 14.4 %all_gather.14 = bf16[64,22,256]{2,0,1:T(8,128)(2,1)} all-gather(bf16[16,22,256]{2,0,1:T(8,128)(2,1)S(1)} %copy.73), channel_id=1, replica_groups=mesh['ep_0'=16,'ep_1'=4,'ep_2'=2,'tp'=4] {'ep_1'}, dimensions={0}, use_global_device_ids=true | all-gather | bytes 901120 | tf_op jit(solution)/shard_map/all_gather | solution.py:46
  88.0 0.2 select_reduce_fusion.1
  88.4 0.2 multiply_reduce_fusion
  88.6 0.7 multiply_convert_fusion
  89.6 1.0 convolution_convert_fusion
  90.6 1.1 broadcast_in_dim.58
  91.7 12.0 %all-to-all-start.1 = ((bf16[128,1,2,1024]{3,2,1,0:T(2,128)(2,1)}), bf16[128,1,2,1024]{3,2,1,0:T(2,128)(2,1)S(1)}, u32[]{:S(2)}, u32[]{:S(2)}) async-start(bf16[128,1,2,1024]{3,2,1,0:T(2,128)(2,1)} %bitcast.5), calls=%async_computation.1 | async-start | bytes 1048576 | tf_op jit(solution)/shard_map/all_to_all | solution.py:176
  103.7 0.1 fusion.16
  103.9 0.1 fusion.17
  104.0 32.8 %all-to-all-done.1 = bf16[128,1,2,1024]{3,2,1,0:T(2,128)(2,1)S(1)} async-done(((bf16[128,1,2,1024]{3,2,1,0:T(2,128)(2,1)}), bf16[128,1,2,1024]{3,2,1,0:T(2,128)(2,1)S(1)}, u32[]{:S(2)}, u32[]{:S(2)}) %all-to-all-start.1) | async-done | bytes 524320 | tf_op jit(solution)/shard_map/all_to_all | solution.py:176
  136.8 0.2 reshape.281
  137.0 0.3 fusion.46
  137.4 0.9 fusion.6
  138.3 0.4 convert_element_type.104
  138.6 1.2 copy.82
  139.8 4.8 %all-to-all-start.2 = ((bf16[4,128,1,2,256]{4,3,1,2,0:T(2,128)(2,1)}), bf16[4,128,1,2,256]{4,3,1,2,0:T(2,128)(2,1)S(1)}, u32[]{:S(2)}, u32[]{:S(2)}) async-start(bf16[4,128,1,2,256]{4,3,1,2,0:T(2,128)(2,1)} %bitcast.80), calls=%async_computation.2 | async-start | bytes 1048576 | tf_op jit(solution)/shard_map/all_to_all | solution.py:33
  144.8 0.2 select_reduce_fusion
  145.0 10.0 %all-to-all-done.2 = bf16[4,128,1,2,256]{4,3,1,2,0:T(2,128)(2,1)S(1)} async-done(((bf16[4,128,1,2,256]{4,3,1,2,0:T(2,128)(2,1)}), bf16[4,128,1,2,256]{4,3,1,2,0:T(2,128)(2,1)S(1)}, u32[]{:S(2)}, u32[]{:S(2)}) %all-to-all-start.2) | async-done | bytes 524320 | tf_op jit(solution)/shard_map/all_to_all | solution.py:33
  155.0 1.3 reduce_sum.121
  156.3 5.8 %all-to-all-start.3 = ((bf16[128,1,2,256]{3,2,1,0:T(2,128)(2,1)}), bf16[128,1,2,256]{3,2,1,0:T(2,128)(2,1)S(1)}, u32[]{:S(2)}, u32[]{:S(2)}) async-start(bf16[128,1,2,256]{3,2,1,0:T(2,128)(2,1)} %bitcast.7), calls=%async_computation.3 | async-start | bytes 262144 | tf_op jit(solution)/shard_map/all_to_all | solution.py:189
  162.3 0.1 fusion.21
  162.4 2.2 copy.81
  164.6 0.4 reshape_reshape.7
  165.1 14.3 %all-to-all-done.3 = bf16[128,1,2,256]{3,2,1,0:T(2,128)(2,1)S(1)} async-done(((bf16[128,1,2,256]{3,2,1,0:T(2,128)(2,1)}), bf16[128,1,2,256]{3,2,1,0:T(2,128)(2,1)S(1)}, u32[]{:S(2)}, u32[]{:S(2)}) %all-to-all-start.3) | async-done | bytes 131104 | tf_op jit(solution)/shard_map/all_to_all | solution.py:189
  179.5 70.4 %all-gather.5.cloned.1.call-done = bf16[1024,1024]{1,0:T(8,128)(2,1)} async-done(((bf16[8,1024]{1,0:T(8,128)(2,1)}), bf16[1024,1024]{1,0:T(8,128)(2,1)}) %all-gather.5.cloned.1.call-update) | async-done | bytes 2097168 | tf_op jit(solution)/shard_map/all_gather | solution.py:204
  249.9 2.4 fusion.47
  252.3 0.7 fusion.8
  253.0 0.9 copy.71
  253.9 12.2 %all-to-all-start.4 = ((bf16[128,8,22]{2,1,0:T(8,128)(2,1)}), bf16[128,8,22]{2,1,0:T(8,128)(2,1)S(1)}, u32[]{:S(2)}, u32[]{:S(2)}) async-start(bf16[128,8,22]{2,1,0:T(8,128)(2,1)} %bitcast.9), calls=%async_computation.4 | async-start | bytes 524288 | tf_op jit(solution)/shard_map/all_to_all | solution.py:208
  266.2 22.4 %all-to-all-done.4 = bf16[128,8,22]{2,1,0:T(8,128)(2,1)S(1)} async-done(((bf16[128,8,22]{2,1,0:T(8,128)(2,1)}), bf16[128,8,22]{2,1,0:T(8,128)(2,1)S(1)}, u32[]{:S(2)}, u32[]{:S(2)}) %all-to-all-start.4) | async-done | bytes 45088 | tf_op jit(solution)/shard_map/all_to_all | solution.py:208
  288.6 0.3 all_to_all.37
  289.0 0.4 fusion.44
  289.5 0.6 broadcast_in_dim.60
  290.1 4.3 %all-to-all-start.5 = ((f32[4,1,16]{2,1,0:T(1,128)}), f32[4,1,16]{2,1,0:T(1,128)S(1)}, u32[]{:S(2)}, u32[]{:S(2)}) async-start(f32[4,1,16]{2,1,0:T(1,128)} %broadcast_in_dim.60), calls=%async_computation.5 | async-start | bytes 4096 | tf_op jit(solution)/shard_map/all_to_all | solution.py:17
  294.4 0.7 pad_maximum_fusion
  295.0 4.6 %all-to-all-done.5 = f32[4,1,16]{2,1,0:T(1,128)S(1)} async-done(((f32[4,1,16]{2,1,0:T(1,128)}), f32[4,1,16]{2,1,0:T(1,128)S(1)}, u32[]{:S(2)}, u32[]{:S(2)}) %all-to-all-start.5) | async-done | bytes 288 | tf_op jit(solution)/shard_map/all_to_all | solution.py:17
  299.7 0.7 multiply_convert_fusion.1
  (83 shorter events, 2.4 us)
Async XLA Ops:
  7.2 26.3 %copy-start = (bf16[128,1024]{1,0:T(8,128)(2,1)S(1)}, bf16[128,1024]{1,0:T(8,128)(2,1)}, u32[]{:S(2)}) copy-start(bf16[128,1024]{1,0:T(8,128)(2,1)} %param.28) | copy-start | bytes 786436
  7.2 25.0 %copy-start.16 = (bf16[8,1,1024,128]{3,2,1,0:T(8,128)(2,1)S(1)}, bf16[8,1,1024,128]{3,2,1,0:T(8,128)(2,1)}, u32[]{:S(2)}) copy-start(bf16[8,1,1024,128]{3,2,1,0:T(8,128)(2,1)} %param.21) | copy-start | bytes 6291460
  32.0 1.6 copy-start.15
  32.2 6.6 %copy-start.10 = (bf16[22,256]{1,0:T(8,128)(2,1)S(1)}, bf16[22,256]{1,0:T(8,128)(2,1)}, u32[]{:S(2)}) copy-start(bf16[22,256]{1,0:T(8,128)(2,1)} %param.37) | copy-start | bytes 33796
  33.3 54.4 %copy-start.12 = (s32[8,2]{0,1:T(2,128)S(1)}, s32[8,2]{0,1:T(2,128)}, u32[]{:S(2)}) copy-start(s32[8,2]{0,1:T(2,128)} %param.31) | copy-start | bytes 196
  33.3 55.0 %copy-start.2 = (bf16[8,1024]{1,0:T(8,128)(2,1)S(1)}, bf16[8,1024]{1,0:T(8,128)(2,1)}, u32[]{:S(2)}) copy-start(bf16[8,1024]{1,0:T(8,128)(2,1)} %param.20) | copy-start | bytes 49156
  33.3 55.3 %copy-start.11 = (f32[1024]{0:T(1024)S(1)}, f32[1024]{0:T(1024)}, u32[]{:S(2)}) copy-start(f32[1024]{0:T(1024)} %param.29) | copy-start | bytes 12292
  34.3 54.0 %all-to-all-start = ((bf16[4,8,1024]{2,1,0:T(8,128)(2,1)}), bf16[4,8,1024]{2,1,0:T(8,128)(2,1)S(1)}, u32[]{:S(2)}, u32[]{:S(2)}) async-start(bf16[4,8,1024]{2,1,0:T(8,128)(2,1)} %broadcast_in_dim.35), calls=%async_computation | async-start | bytes 131072 | tf_op jit(solution)/shard_map/all_to_all | solution.py:17
  38.8 123.7 %all-gather.7.cloned.1.call-start = ((), (), s32[]{:S(2)}) async-start(), calls=%async_computation.7 | async-start | bytes 2162688 | tf_op jit(solution)/shard_map/all_gather | solution.py:46
  73.2 30.5 %copy-start.5 = (bf16[1024,64]{0,1:T(8,128)(2,1)S(1)}, bf16[1024,64]{0,1:T(8,128)(2,1)}, u32[]{:S(2)}) copy-start(bf16[1024,64]{0,1:T(8,128)(2,1)} %param.24) | copy-start | bytes 393220
  73.2 30.7 %copy-start.6 = (bf16[1024,64]{0,1:T(8,128)(2,1)S(1)}, bf16[1024,64]{0,1:T(8,128)(2,1)}, u32[]{:S(2)}) copy-start(bf16[1024,64]{0,1:T(8,128)(2,1)} %param.25) | copy-start | bytes 393220
  87.7 49.4 %copy-start.4 = (bf16[1024,112]{0,1:T(8,128)(2,1)S(1)}, bf16[1024,112]{0,1:T(8,128)(2,1)}, u32[]{:S(2)}) copy-start(bf16[1024,112]{0,1:T(8,128)(2,1)} %param.32) | copy-start | bytes 688132
  87.7 162.3 %all-gather.5.cloned.1.call-start = ((), (), s32[]{:S(2)}) async-start(), calls=%async_computation.6 | async-start | bytes 2113536 | tf_op jit(solution)/shard_map/all_gather | solution.py:204
  89.6 47.8 %copy-start.17 = (bf16[112,1024]{1,0:T(8,128)(2,1)S(1)}, bf16[112,1024]{1,0:T(8,128)(2,1)}, u32[]{:S(2)}) copy-start(bf16[112,1024]{1,0:T(8,128)(2,1)} %param.34) | copy-start | bytes 688132
  89.6 47.8 %copy-start.18 = (bf16[1024,112]{0,1:T(8,128)(2,1)S(1)}, bf16[1024,112]{0,1:T(8,128)(2,1)}, u32[]{:S(2)}) copy-start(bf16[1024,112]{0,1:T(8,128)(2,1)} %param.33) | copy-start | bytes 688132
  91.7 45.1 %all-to-all-start.1 = ((bf16[128,1,2,1024]{3,2,1,0:T(2,128)(2,1)}), bf16[128,1,2,1024]{3,2,1,0:T(2,128)(2,1)S(1)}, u32[]{:S(2)}, u32[]{:S(2)}) async-start(bf16[128,1,2,1024]{3,2,1,0:T(2,128)(2,1)} %bitcast.5), calls=%async_computation.1 | async-start | bytes 1048576 | tf_op jit(solution)/shard_map/all_to_all | solution.py:176
  137.4 7.3 %copy-start.13 = (bf16[1024]{0:T(1024)(128)(2,1)S(1)}, bf16[1024]{0:T(1024)(128)(2,1)}, u32[]{:S(2)}) copy-start(bf16[1024]{0:T(1024)(128)(2,1)} %param.38) | copy-start | bytes 6148
  137.4 7.3 %copy-start.3 = (bf16[8,1024]{1,0:T(8,128)(2,1)S(1)}, bf16[8,1024]{1,0:T(8,128)(2,1)}, u32[]{:S(2)}) copy-start(bf16[8,1024]{1,0:T(8,128)(2,1)} %multiply_convert_fusion) | copy-start | bytes 49156
  137.4 7.3 %copy-start.9 = (bf16[1024,16]{0,1:T(8,128)(2,1)S(1)}, bf16[1024,16]{0,1:T(8,128)(2,1)}, u32[]{:S(2)}) copy-start(bf16[1024,16]{0,1:T(8,128)(2,1)} %param.30) | copy-start | bytes 98308
  139.8 15.1 %all-to-all-start.2 = ((bf16[4,128,1,2,256]{4,3,1,2,0:T(2,128)(2,1)}), bf16[4,128,1,2,256]{4,3,1,2,0:T(2,128)(2,1)S(1)}, u32[]{:S(2)}, u32[]{:S(2)}) async-start(bf16[4,128,1,2,256]{4,3,1,2,0:T(2,128)(2,1)} %bitcast.80), calls=%async_computation.2 | async-start | bytes 1048576 | tf_op jit(solution)/shard_map/all_to_all | solution.py:33
  156.3 23.0 %all-to-all-start.3 = ((bf16[128,1,2,256]{3,2,1,0:T(2,128)(2,1)}), bf16[128,1,2,256]{3,2,1,0:T(2,128)(2,1)S(1)}, u32[]{:S(2)}, u32[]{:S(2)}) async-start(bf16[128,1,2,256]{3,2,1,0:T(2,128)(2,1)} %bitcast.7), calls=%async_computation.3 | async-start | bytes 262144 | tf_op jit(solution)/shard_map/all_to_all | solution.py:189
  164.6 85.3 %copy-start.7 = (bf16[1024,22]{0,1:T(8,128)(2,1)S(1)}, bf16[1024,22]{0,1:T(8,128)(2,1)}, u32[]{:S(2)}) copy-start(bf16[1024,22]{0,1:T(8,128)(2,1)} %param.35) | copy-start | bytes 135172
  165.1 87.2 %copy-start.8 = (bf16[1024,22]{0,1:T(8,128)(2,1)S(1)}, bf16[1024,22]{0,1:T(8,128)(2,1)}, u32[]{:S(2)}) copy-start(bf16[1024,22]{0,1:T(8,128)(2,1)} %param.36) | copy-start | bytes 135172
  249.9 2.4 copy-start.1
  253.0 46.7 %copy-start.14 = (f32[256]{0:T(256)S(1)}, f32[256]{0:T(256)}, u32[]{:S(2)}) copy-start(f32[256]{0:T(256)} %param.39) | copy-start | bytes 3076
  253.9 34.7 %all-to-all-start.4 = ((bf16[128,8,22]{2,1,0:T(8,128)(2,1)}), bf16[128,8,22]{2,1,0:T(8,128)(2,1)S(1)}, u32[]{:S(2)}, u32[]{:S(2)}) async-start(bf16[128,8,22]{2,1,0:T(8,128)(2,1)} %bitcast.9), calls=%async_computation.4 | async-start | bytes 524288 | tf_op jit(solution)/shard_map/all_to_all | solution.py:208
  290.1 9.5 %all-to-all-start.5 = ((f32[4,1,16]{2,1,0:T(1,128)}), f32[4,1,16]{2,1,0:T(1,128)S(1)}, u32[]{:S(2)}, u32[]{:S(2)}) async-start(f32[4,1,16]{2,1,0:T(1,128)} %broadcast_in_dim.60), calls=%async_computation.5 | async-start | bytes 4096 | tf_op jit(solution)/shard_map/all_to_all | solution.py:17
Sparse Core Ops, SparseCore 0:
  87.8 17.4 all-gather.6
  108.4 141.4 all-gather.4
where the time goes:
time: 308 us; the launch traced here: 307 us
  waiting for transfers between devices  154 us (50%)
  blocking collectives  48.8 us (16%)
  starting transfers between devices  43.6 us (14%)
  other arithmetic  25.7 us (8%)
  between operations  14.5 us (5%)
  matrix products  11.1 us (4%)
  local copies, waits for them, and re-layouts  9.16 us (3%)
    all_gather x1, waiting for transfers between devices, body(): shard_rows = lax.all_gather(settled, EP, axis=0, tiled=True)  70.4 us
    all_gather x2, blocking collectives, stacked_from(): tiles = lax.all_gather(tiles, axes[k], axis=0, tiled=True)  48.8 us
    all_to_all x1, waiting for transfers between devices, body(): lax.all_to_all(outgoing, EP, split_axis=0, concat_axis=0, tiled=True)  32.8 us
    all_to_all x1, waiting for transfers between devices, body(): lax.all_to_all(dense_hidden, EP, split_axis=0, concat_axis=1, tiled=True)  22.4 us
    another operation x2, other arithmetic  20.1 us
    all_to_all x1, waiting for transfers between devices, body(): lax.all_to_all(summed.astype(jnp.bfloat16), EP, split_axis=0, concat_axis...  14.3 us
    all_to_all x1, starting transfers between devices, body(): lax.all_to_all(dense_hidden, EP, split_axis=0, concat_axis=1, tiled=True)  12.2 us
    all_to_all x1, starting transfers between devices, body(): lax.all_to_all(outgoing, EP, split_axis=0, concat_axis=0, tiled=True)  12 us
  transfers between devices with their start and end apart: 8, of which 6 were waited for; matrix products, arithmetic and copies ran while one was open for 4% of the time, Pallas kernels for 0%

commit v1 on v0

--- a/solution.py
+++ b/solution.py
@@ -201,7 +201,9 @@
     routed = jnp.dot(weighted, gathered, precision=PRECISE)
     column_rank = lax.axis_index("tp")
     own_settled = lax.dynamic_slice_in_dim(settled, column_rank * slice_width, slice_width, 1)
-    shard_rows = lax.all_gather(settled, EP, axis=0, tiled=True)
+    shard_rows = jnp.concatenate(
+        lax.all_to_all(jnp.stack([settled] * lax.axis_size(EP)), EP, 0, 0), axis=0
+    )
     gate_pre = jnp.dot(shard_rows, dense_gate, preferred_element_type=jnp.float32)
     up_pre = jnp.dot(shard_rows, dense_up, preferred_element_type=jnp.float32)
     dense_hidden = (jax.nn.silu(gate_pre) * up_pre).astype(jnp.bfloat16)

time: 308 us -> 363 us (1.18)
  blocking collectives: 48.8 us -> 165 us
  waiting for transfers between devices: 154 us -> 82.2 us
  starting transfers between devices: 43.6 us -> 50.4 us
  local copies, waits for them, and re-layouts: 9.16 us -> 14 us
    all_gather x2, blocking collectives: 48.8 us -> 130 us  [stacked_from(): tiles = lax.all_gather(tiles, axes[k], axis=0, tiled=True)]
    all_gather x1 -> x0, waiting for transfers between devices: 70.4 us -> none  [body(): shard_rows = lax.all_gather(settled, EP, axis=0, tiled=True)]
    all_to_all x0 -> x2, blocking collectives: none -> 35.8 us  [the longest x1 22.8 us: body(): lax.all_to_all(summed.astype(jnp.bfloat16), EP, split_axis=0, concat_axis...]
    all_to_all x2 -> x1, waiting for transfers between devices: 24.2 us -> 0.01 us  [body(): lax.all_to_all(jnp.stack([settled] * lax.axis_size(EP)), EP, 0, 0)]
    all_gather x1, waiting for transfers between devices: 0.01 us -> 17.3 us  [stacked_from(): tiles = lax.all_gather(tiles, axes[k], axis=0, tiled=True)]
    all_to_all x1, starting transfers between devices: 12 us -> 19 us  [body(): lax.all_to_all(outgoing, EP, split_axis=0, concat_axis=0, tiled=True)]
    all_to_all x2, waiting for transfers between devices: 4.56 us -> 9.37 us  [from_everyone(): return lax.all_to_all(copies, axis, split_axis=0, concat_axis=0, tiled=True)]
    all_to_all x2 -> x1, starting transfers between devices: 10.6 us -> 6.2 us  [body(): lax.all_to_all(jnp.stack([settled] * lax.axis_size(EP)), EP, 0, 0)]
  transfers between devices with their start and end apart: 8 -> 6, of which waited for: 6 -> 5; matrix products, arithmetic and copies ran while one was open for 4% -> 3% of each run, Pallas kernels for 0% -> 0%
where the time goes in v1:
time: 363 us; the launch traced here: 362 us
  blocking collectives  165 us (45%)
  waiting for transfers between devices  82.2 us (23%)
  starting transfers between devices  50.4 us (14%)
  other arithmetic  24.4 us (7%)
  between operations  14.4 us (4%)
  local copies, waits for them, and re-layouts  14 us (4%)
  matrix products  11.6 us (3%)
    all_gather x2, blocking collectives, stacked_from(): tiles = lax.all_gather(tiles, axes[k], axis=0, tiled=True)  130 us
    all_to_all x1, waiting for transfers between devices, body(): lax.all_to_all(outgoing, EP, split_axis=0, concat_axis=0, tiled=True)  33.1 us
    all_to_all x1, blocking collectives, body(): lax.all_to_all(summed.astype(jnp.bfloat16), EP, split_axis=0, concat_axis...  22.8 us
    all_to_all x1, waiting for transfers between devices, body(): lax.all_to_all(dense_hidden, EP, split_axis=0, concat_axis=1, tiled=True)  22.4 us
    another operation x2, other arithmetic  20.1 us
    all_to_all x1, starting transfers between devices, body(): lax.all_to_all(outgoing, EP, split_axis=0, concat_axis=0, tiled=True)  19 us
    all_gather x1, waiting for transfers between devices, stacked_from(): tiles = lax.all_gather(tiles, axes[k], axis=0, tiled=True)  17.3 us
    all_to_all x1, starting transfers between devices, body(): lax.all_to_all(dense_hidden, EP, split_axis=0, concat_axis=1, tiled=True)  16.4 us
  transfers between devices with their start and end apart: 6, of which 5 were waited for; matrix products, arithmetic and copies ran while one was open for 3% of the time, Pallas kernels for 0%

profile of v1, /device:TPU:32, one launch (start us, length us, event | category | flops | bytes accessed | tf_op | source)
XLA Modules:
  0.0 362.5 jit_solution(17378950936821138203)
XLA Ops:
  7.2 0.8 iota_compare_fusion
  8.0 1.1 convolution_convert_fusion.4
  9.1 2.3 fusion.40
  11.5 19.8 %reduce-window.6 = f32[8,1,2,8,128]{4,3,2,1,0:T(8,128)S(1)} reduce-window(f32[8,1,2,8,128]{4,3,2,1,0:T(8,128)S(1)} %bitcast.97, f32[]{:T(128)} %constant.108.clone.1), window={size=1x1x1x1x128 pad=0_0x0_0x0_0x0_0x0_127}, to_apply=%region_0.1 | reduce-window | flops 2080768 | bytes 131076 | tf_op jit(solution)/shard_map/reduce-window
  31.4 0.2 copy.65
  31.5 0.3 reduce-window.9
  32.1 2.7 multiply_reduce_fusion.3
  35.0 0.2 convolution_convert_fusion.1
  35.2 0.6 broadcast_in_dim.35
  35.8 4.5 %all-to-all-start = ((bf16[4,8,1024]{2,1,0:T(8,128)(2,1)}), bf16[4,8,1024]{2,1,0:T(8,128)(2,1)S(1)}, u32[]{:S(2)}, u32[]{:S(2)}) async-start(bf16[4,8,1024]{2,1,0:T(8,128)(2,1)} %broadcast_in_dim.35), calls=%async_computation | async-start | bytes 131072 | tf_op jit(solution)/shard_map/all_to_all | solution.py:17
  40.5 0.2 select_reduce_fusion.1
  41.1 4.8 %all-to-all-done = bf16[4,8,1024]{2,1,0:T(8,128)(2,1)S(1)} async-done(((bf16[4,8,1024]{2,1,0:T(8,128)(2,1)}), bf16[4,8,1024]{2,1,0:T(8,128)(2,1)S(1)}, u32[]{:S(2)}, u32[]{:S(2)}) %all-to-all-start) | async-done | bytes 65568 | tf_op jit(solution)/shard_map/all_to_all | solution.py:17
  46.0 0.2 multiply_reduce_fusion
  46.3 0.2 convolution_convert_fusion
  46.6 1.1 broadcast_in_dim.58
  47.6 19.0 %all-to-all-start.1 = ((bf16[128,1,2,1024]{3,2,1,0:T(2,128)(2,1)}), bf16[128,1,2,1024]{3,2,1,0:T(2,128)(2,1)S(1)}, u32[]{:S(2)}, u32[]{:S(2)}) async-start(bf16[128,1,2,1024]{3,2,1,0:T(2,128)(2,1)} %bitcast.5), calls=%async_computation.1 | async-start | bytes 1048576 | tf_op jit(solution)/shard_map/all_to_all | solution.py:176
  66.7 33.1 %all-to-all-done.1 = bf16[128,1,2,1024]{3,2,1,0:T(2,128)(2,1)S(1)} async-done(((bf16[128,1,2,1024]{3,2,1,0:T(2,128)(2,1)}), bf16[128,1,2,1024]{3,2,1,0:T(2,128)(2,1)S(1)}, u32[]{:S(2)}, u32[]{:S(2)}) %all-to-all-start.1) | async-done | bytes 524320 | tf_op jit(solution)/shard_map/all_to_all | solution.py:176
  99.8 0.2 reshape.286
  100.0 0.3 fusion.55
  100.3 0.9 fusion.10
  101.2 0.4 convert_element_type.104
  101.6 0.4 copy.82
  102.0 13.0 %all_to_all.50 = bf16[4,128,1,2,256]{4,3,1,2,0:T(2,128)(2,1)S(1)} all-to-all(bf16[4,128,1,2,256]{4,3,1,2,0:T(2,128)(2,1)S(1)} %bitcast.90), channel_id=1, replica_groups=mesh['ep_0'=16,'ep_1'=4,'ep_2'=2,'tp'=4] {'tp'}, dimensions={0} | all-to-all | bytes 1048576 | tf_op jit(solution)/shard_map/all_to_all | solution.py:33
  115.0 0.7 reduce_sum.121
  115.7 22.8 %all_to_all.51 = bf16[128,1,2,256]{3,2,1,0:T(2,128)(2,1)S(1)} all-to-all(bf16[128,1,2,256]{3,2,1,0:T(2,128)(2,1)S(1)} %bitcast.96), channel_id=1, replica_groups=mesh['ep_0'=16,'ep_1'=4,'ep_2'=2,'tp'=4] {'ep_0','ep_1','ep_2'}, dimensions={0} | all-to-all | bytes 262144 | tf_op jit(solution)/shard_map/all_to_all | solution.py:189
  138.4 1.6 stack.2
  140.1 6.2 %all-to-all-start.4 = ((bf16[128,8,1024]{2,1,0:T(8,128)(2,1)}), bf16[128,8,1024]{2,1,0:T(8,128)(2,1)S(1)}, u32[]{:S(2)}, u32[]{:S(2)}) async-start(bf16[128,8,1024]{2,1,0:T(8,128)(2,1)} %stack.2), calls=%async_computation.4 | async-start | bytes 4194304 | tf_op jit(solution)/shard_map/all_to_all | solution.py:205
  146.4 115.0 %all-gather.1 = bf16[16,22,256]{2,1,0:T(8,128)(2,1)S(1)} all-gather(bf16[1,22,256]{2,1,0:T(8,128)(2,1)S(1)} %bitcast.99), channel_id=2, replica_groups=mesh['ep_0'=16,'ep_1'=4,'ep_2'=2,'tp'=4] {'ep_0'}, dimensions={0}, use_global_device_ids=true | all-gather | bytes 191488 | tf_op jit(solution)/shard_map/all_gather | solution.py:46
  261.4 14.7 %all_gather.10 = bf16[64,22,256]{2,0,1:T(8,128)(2,1)} all-gather(bf16[16,22,256]{2,0,1:T(8,128)(2,1)S(1)} %copy.73), channel_id=1, replica_groups=mesh['ep_0'=16,'ep_1'=4,'ep_2'=2,'tp'=4] {'ep_1'}, dimensions={0}, use_global_device_ids=true | all-gather | bytes 901120 | tf_op jit(solution)/shard_map/all_gather | solution.py:46
  276.2 0.1 fusion.25
  276.3 0.1 fusion.26
  276.5 0.1 fusion.54
  276.6 0.2 select_reduce_fusion
  277.1 17.3 %all-gather.4.cloned.1.call-done = bf16[128,22,256]{2,0,1:T(8,128)(2,1)} async-done(((bf16[64,22,256]{2,0,1:T(8,128)(2,1)}), bf16[128,22,256]{2,0,1:T(8,128)(2,1)}) %all-gather.4.cloned.1.call-update) | async-done | bytes 1441808 | tf_op jit(solution)/shard_map/all_gather | solution.py:46
  294.5 3.3 copy.81
  297.8 3.4 reshape_reshape.7
  301.4 0.7 fusion.6
  302.0 0.7 fusion.15
  302.7 0.9 copy.71
  303.6 16.4 %all-to-all-start.5 = ((bf16[128,8,22]{2,1,0:T(8,128)(2,1)}), bf16[128,8,22]{2,1,0:T(8,128)(2,1)S(1)}, u32[]{:S(2)}, u32[]{:S(2)}) async-start(bf16[128,8,22]{2,1,0:T(8,128)(2,1)} %bitcast.10), calls=%async_computation.5 | async-start | bytes 524288 | tf_op jit(solution)/shard_map/all_to_all | solution.py:210
  320.1 22.4 %all-to-all-done.5 = bf16[128,8,22]{2,1,0:T(8,128)(2,1)S(1)} async-done(((bf16[128,8,22]{2,1,0:T(8,128)(2,1)}), bf16[128,8,22]{2,1,0:T(8,128)(2,1)S(1)}, u32[]{:S(2)}, u32[]{:S(2)}) %all-to-all-start.5) | async-done | bytes 45088 | tf_op jit(solution)/shard_map/all_to_all | solution.py:210
  342.5 0.3 all_to_all.41
  342.9 1.8 fusion.53
  344.8 0.6 broadcast_in_dim.60
  345.4 4.3 %all-to-all-start.6 = ((f32[4,1,16]{2,1,0:T(1,128)}), f32[4,1,16]{2,1,0:T(1,128)S(1)}, u32[]{:S(2)}, u32[]{:S(2)}) async-start(f32[4,1,16]{2,1,0:T(1,128)} %broadcast_in_dim.60), calls=%async_computation.6 | async-start | bytes 4096 | tf_op jit(solution)/shard_map/all_to_all | solution.py:17
  349.6 0.7 pad_maximum_fusion
  350.3 4.6 %all-to-all-done.6 = f32[4,1,16]{2,1,0:T(1,128)S(1)} async-done(((f32[4,1,16]{2,1,0:T(1,128)}), f32[4,1,16]{2,1,0:T(1,128)S(1)}, u32[]{:S(2)}, u32[]{:S(2)}) %all-to-all-start.6) | async-done | bytes 288 | tf_op jit(solution)/shard_map/all_to_all | solution.py:17
  354.9 0.7 multiply_convert_fusion.1
  (75 shorter events, 2.4 us)
Async XLA Ops:
  7.2 27.8 %copy-start = (bf16[128,1024]{1,0:T(8,128)(2,1)S(1)}, bf16[128,1024]{1,0:T(8,128)(2,1)}, u32[]{:S(2)}) copy-start(bf16[128,1024]{1,0:T(8,128)(2,1)} %param.28) | copy-start | bytes 786436
  31.8 3.2 copy-start.13
  32.1 8.2 %copy-start.10 = (s32[8,2]{0,1:T(2,128)S(1)}, s32[8,2]{0,1:T(2,128)}, u32[]{:S(2)}) copy-start(s32[8,2]{0,1:T(2,128)} %param.31) | copy-start | bytes 196
  32.1 13.8 %copy-start.1 = (bf16[8,1024]{1,0:T(8,128)(2,1)S(1)}, bf16[8,1024]{1,0:T(8,128)(2,1)}, u32[]{:S(2)}) copy-start(bf16[8,1024]{1,0:T(8,128)(2,1)} %param.20) | copy-start | bytes 49156
  32.1 14.2 %copy-start.9 = (f32[1024]{0:T(1024)S(1)}, f32[1024]{0:T(1024)}, u32[]{:S(2)}) copy-start(f32[1024]{0:T(1024)} %param.29) | copy-start | bytes 12292
  34.8 65.2 %copy-start.2 = (bf16[1024,112]{0,1:T(8,128)(2,1)S(1)}, bf16[1024,112]{0,1:T(8,128)(2,1)}, u32[]{:S(2)}) copy-start(bf16[1024,112]{0,1:T(8,128)(2,1)} %param.32) | copy-start | bytes 688132
  35.8 10.1 %all-to-all-start = ((bf16[4,8,1024]{2,1,0:T(8,128)(2,1)}), bf16[4,8,1024]{2,1,0:T(8,128)(2,1)S(1)}, u32[]{:S(2)}, u32[]{:S(2)}) async-start(bf16[4,8,1024]{2,1,0:T(8,128)(2,1)} %broadcast_in_dim.35), calls=%async_computation | async-start | bytes 131072 | tf_op jit(solution)/shard_map/all_to_all | solution.py:17
  41.0 59.3 %copy-start.14 = (bf16[112,1024]{1,0:T(8,128)(2,1)S(1)}, bf16[112,1024]{1,0:T(8,128)(2,1)}, u32[]{:S(2)}) copy-start(bf16[112,1024]{1,0:T(8,128)(2,1)} %param.34) | copy-start | bytes 688132
  41.0 59.3 %copy-start.15 = (bf16[1024,112]{0,1:T(8,128)(2,1)S(1)}, bf16[1024,112]{0,1:T(8,128)(2,1)}, u32[]{:S(2)}) copy-start(bf16[1024,112]{0,1:T(8,128)(2,1)} %param.33) | copy-start | bytes 688132
  47.6 52.2 %all-to-all-start.1 = ((bf16[128,1,2,1024]{3,2,1,0:T(2,128)(2,1)}), bf16[128,1,2,1024]{3,2,1,0:T(2,128)(2,1)S(1)}, u32[]{:S(2)}, u32[]{:S(2)}) async-start(bf16[128,1,2,1024]{3,2,1,0:T(2,128)(2,1)} %bitcast.5), calls=%async_computation.1 | async-start | bytes 1048576 | tf_op jit(solution)/shard_map/all_to_all | solution.py:176
  140.1 6.3 %copy-start.8 = (bf16[22,256]{1,0:T(8,128)(2,1)S(1)}, bf16[22,256]{1,0:T(8,128)(2,1)}, u32[]{:S(2)}) copy-start(bf16[22,256]{1,0:T(8,128)(2,1)} %param.37) | copy-start | bytes 33796
  140.1 161.3 %all-to-all-start.4 = ((bf16[128,8,1024]{2,1,0:T(8,128)(2,1)}), bf16[128,8,1024]{2,1,0:T(8,128)(2,1)S(1)}, u32[]{:S(2)}, u32[]{:S(2)}) async-start(bf16[128,8,1024]{2,1,0:T(8,128)(2,1)} %stack.2), calls=%async_computation.4 | async-start | bytes 4194304 | tf_op jit(solution)/shard_map/all_to_all | solution.py:205
  146.3 129.9 %copy-start.11 = (bf16[1024]{0:T(1024)(128)(2,1)S(1)}, bf16[1024]{0:T(1024)(128)(2,1)}, u32[]{:S(2)}) copy-start(bf16[1024]{0:T(1024)(128)(2,1)} %param.38) | copy-start | bytes 6148
  146.3 129.9 %copy-start.3 = (bf16[1024,64]{0,1:T(8,128)(2,1)S(1)}, bf16[1024,64]{0,1:T(8,128)(2,1)}, u32[]{:S(2)}) copy-start(bf16[1024,64]{0,1:T(8,128)(2,1)} %param.24) | copy-start | bytes 393220
  146.3 130.0 %copy-start.4 = (bf16[1024,64]{0,1:T(8,128)(2,1)S(1)}, bf16[1024,64]{0,1:T(8,128)(2,1)}, u32[]{:S(2)}) copy-start(bf16[1024,64]{0,1:T(8,128)(2,1)} %param.25) | copy-start | bytes 393220
  146.3 130.2 %copy-start.7 = (bf16[1024,16]{0,1:T(8,128)(2,1)S(1)}, bf16[1024,16]{0,1:T(8,128)(2,1)}, u32[]{:S(2)}) copy-start(bf16[1024,16]{0,1:T(8,128)(2,1)} %param.30) | copy-start | bytes 98308
  146.3 148.1 %all-gather.4.cloned.1.call-start = ((), (), s32[]{:S(2)}) async-start(), calls=%async_computation.7 | async-start | bytes 2162688 | tf_op jit(solution)/shard_map/all_gather | solution.py:46
  297.8 3.6 copy-start.5
  301.2 0.8 copy-start.6
  302.7 52.3 %copy-start.12 = (f32[256]{0:T(256)S(1)}, f32[256]{0:T(256)}, u32[]{:S(2)}) copy-start(f32[256]{0:T(256)} %param.39) | copy-start | bytes 3076
  303.6 38.9 %all-to-all-start.5 = ((bf16[128,8,22]{2,1,0:T(8,128)(2,1)}), bf16[128,8,22]{2,1,0:T(8,128)(2,1)S(1)}, u32[]{:S(2)}, u32[]{:S(2)}) async-start(bf16[128,8,22]{2,1,0:T(8,128)(2,1)} %bitcast.10), calls=%async_computation.5 | async-start | bytes 524288 | tf_op jit(solution)/shard_map/all_to_all | solution.py:210
  345.4 9.5 %all-to-all-start.6 = ((f32[4,1,16]{2,1,0:T(1,128)}), f32[4,1,16]{2,1,0:T(1,128)S(1)}, u32[]{:S(2)}, u32[]{:S(2)}) async-start(f32[4,1,16]{2,1,0:T(1,128)} %broadcast_in_dim.60), calls=%async_computation.6 | async-start | bytes 4096 | tf_op jit(solution)/shard_map/all_to_all | solution.py:17
Sparse Core Ops, SparseCore 0:
  276.2 18.1 all-gather.3
